TPU v7x, 32 devices: a whole 2x2x4 slice. The times are simulated.
32 devices in a mesh: kv: 8 (over z, y), tp: 4 (over x, core).
Axes of the slice: x: 2, y: 2, z: 4, core: 2. Of those that a mesh axis runs over, the one named last changes fastest.
Arguments:
- stream: bfloat16 [24, 4096], P(None, ('kv', 'tp')), may hold values from -50 to 50
- attention_gain: float32 [4096], P(('kv', 'tp')), may hold values from 0.1 to 1.9
- query_down: bfloat16 [4096, 1536], P(('kv', 'tp')), may hold values from -0.09375 to 0.09375
- latent_down: bfloat16 [4096, 512], P(('kv', 'tp')), may hold values from -0.09375 to 0.09375
- rotary_down: bfloat16 [4096, 64], P(('kv', 'tp')), may hold values from -0.1875 to 0.1875
- query_gain: float32 [1536], replicated, may hold values from 0.1 to 1.9
- latent_gain: float32 [512], replicated, may hold values from 0.1 to 1.9
- query_content: bfloat16 [1536, 2048], P(None, 'tp'), may hold values from -0.15625 to 0.15625
- query_rotary: bfloat16 [1536, 1024], P(None, 'tp'), may hold values from -0.15625 to 0.15625
- key_absorb: bfloat16 [16, 128, 512], P('tp'), may hold values from -0.5 to 0.5
- value_absorb: bfloat16 [16, 512, 128], P('tp'), may hold values from -0.25 to 0.25
- latent_cache: bfloat16 [24, 2048, 512], P(None, 'kv'), may hold values from -1200 to 1200
- rotary_cache: bfloat16 [24, 2048, 64], P(None, 'kv'), may hold values from -5 to 5
- head_gain: float32 [2048], P('tp'), may hold values from 0.1 to 1.9
- output_weight: bfloat16 [2048, 4096], P('tp', 'kv'), may hold values from -0.125 to 0.125
- mixer_gain: float32 [4096], P('kv'), may hold values from 0.1 to 1.9
- gate_weight: bfloat16 [4096, 11264], P('kv', 'tp'), may hold values from -0.09375 to 0.09375
- up_weight: bfloat16 [4096, 11264], P('kv', 'tp'), may hold values from -0.09375 to 0.09375
- down_weight: bfloat16 [11264, 4096], P('tp', 'kv'), may hold values from -0.0546875 to 0.0546875
Outputs:
- stream_out: bfloat16 [24, 4096], P(None, ('kv', 'tp'))
All inputs are finite; a program needn't handle non-finite values.
Results may differ from a plain program's by a relative error of at most 0.018.
Values may be sent and summed in bfloat16 or wider, within the bound.
A program may use at most 64 MiB of HBM per device.

v0:
```python
import jax
import jax.numpy as jnp
from jax import lax
from jax.sharding import PartitionSpec as P

epsilon = 1e-06
rope_base = 10000.0


def rotate(values, position):
    half = values.shape[-1] // 2
    freqs = rope_base ** (-jnp.arange(half, dtype=jnp.float32) * 2.0 / values.shape[-1])
    angle = position * freqs
    cosine = jnp.cos(angle)
    sine = jnp.sin(angle)
    first = values[..., :half]
    second = values[..., half:]
    return jnp.concatenate(
        [first * cosine - second * sine, second * cosine + first * sine], axis=-1
    )


def inv_rms(values):
    return lax.rsqrt(jnp.mean(values * values, axis=-1) + epsilon)


def sum_squares(values):
    return jnp.sum(values * values, axis=-1)


def matmul(left, right):
    return jnp.dot(left, right, preferred_element_type=jnp.float32)


def local(
    stream,
    attention_gain,
    query_down,
    latent_down,
    rotary_down,
    query_gain,
    latent_gain,
    query_content,
    query_rotary,
    key_absorb,
    value_absorb,
    latent_cache,
    rotary_cache,
    head_gain,
    output_weight,
    mixer_gain,
    gate_weight,
    up_weight,
    down_weight,
):
    kv_count = lax.axis_size("kv")
    tp_count = lax.axis_size("tp")
    batch_rows = stream.shape[0]
    model_width = stream.shape[1] * kv_count * tp_count
    position = jnp.float32(latent_cache.shape[1] * kv_count)
    stream_block = lax.all_gather(stream, "tp", axis=1, tiled=True)
    stream_f = stream.astype(jnp.float32)
    first_scaled = (stream_f * attention_gain).astype(jnp.bfloat16)
    query_sum, latent_sum, rotary_sum, square_sum = lax.psum(
        (
            matmul(first_scaled, query_down),
            matmul(first_scaled, latent_down),
            matmul(first_scaled, rotary_down),
            sum_squares(stream_f),
        ),
        ("kv", "tp"),
    )
    first_scale = lax.rsqrt(square_sum / model_width + epsilon)[:, None]
    query_low = first_scale * query_sum
    latent_new = first_scale * latent_sum
    rotary_new = first_scale * rotary_sum
    query_normed = (query_low * inv_rms(query_low)[:, None] * query_gain).astype(jnp.bfloat16)
    latent_row = (latent_new * inv_rms(latent_new)[:, None] * latent_gain).astype(jnp.bfloat16)
    rotary_row = rotate(rotary_new, position).astype(jnp.bfloat16)
    heads_here = key_absorb.shape[0]
    query_plain = matmul(query_normed, query_content).astype(jnp.bfloat16)
    query_plain = query_plain.reshape(batch_rows, heads_here, key_absorb.shape[1])
    query_turned = matmul(query_normed, query_rotary).reshape(
        batch_rows, heads_here, rotary_cache.shape[2]
    )
    query_turned = rotate(query_turned, position).astype(jnp.bfloat16)
    query_latent = jnp.einsum(
        "bhn,hnc->bhc", query_plain, key_absorb, preferred_element_type=jnp.float32
    ).astype(jnp.bfloat16)
    scale = (key_absorb.shape[1] + rotary_cache.shape[2]) ** (-0.5)
    scores = (
        jnp.einsum("bhc,bpc->bhp", query_latent, latent_cache, preferred_element_type=jnp.float32)
        + jnp.einsum("bhr,bpr->bhp", query_turned, rotary_cache, preferred_element_type=jnp.float32)
    ) * scale
    maxima = jnp.max(scores, axis=-1)
    expo = jnp.exp(scores - maxima[..., None])
    totals = jnp.sum(expo, axis=-1)
    weighted = jnp.einsum(
        "bhp,bpc->bhc", expo.astype(jnp.bfloat16), latent_cache, preferred_element_type=jnp.float32
    ).astype(jnp.bfloat16)
    all_maxima, all_totals = (
        lax.all_gather(maxima[None], "kv", axis=0, tiled=True),
        lax.all_gather(totals[None], "kv", axis=0, tiled=True),
    )
    own_score = (
        jnp.sum(
            query_latent.astype(jnp.float32) * latent_row.astype(jnp.float32)[:, None, :], axis=-1
        )
        + jnp.sum(
            query_turned.astype(jnp.float32) * rotary_row.astype(jnp.float32)[:, None, :], axis=-1
        )
    ) * scale
    largest = jnp.maximum(jnp.max(all_maxima, axis=0), own_score)
    factors = jnp.exp(all_maxima - largest[None])
    own_weight = jnp.exp(own_score - largest)
    denominator = jnp.sum(factors * all_totals, axis=0) + own_weight
    merged = jnp.sum(
        factors[..., None]
        * lax.all_gather(weighted[None], "kv", axis=0, tiled=True).astype(jnp.float32),
        axis=0,
    )
    merged = merged + own_weight[..., None] * latent_row.astype(jnp.float32)[:, None, :]
    latent_mix = (merged / denominator[..., None]).astype(jnp.bfloat16)
    head_values = jnp.einsum(
        "bhc,hcv->bhv", latent_mix, value_absorb, preferred_element_type=jnp.float32
    ).astype(jnp.bfloat16)
    head_f = head_values.reshape(batch_rows, heads_here * value_absorb.shape[2]).astype(jnp.float32)
    head_square = lax.psum(sum_squares(head_f), "tp")
    head_scale = lax.rsqrt(head_square / (head_f.shape[1] * tp_count) + epsilon)[:, None]
    head_scaled = (head_f * head_gain).astype(jnp.bfloat16)
    attended = lax.psum(matmul(head_scaled, output_weight).astype(jnp.bfloat16), "tp").astype(
        jnp.float32
    )
    middle = (stream_block.astype(jnp.float32) + head_scale * attended).astype(jnp.bfloat16)
    middle_f = middle.astype(jnp.float32)
    second_scaled = (middle_f * mixer_gain).astype(jnp.bfloat16)
    gate_part = matmul(second_scaled, gate_weight)
    up_part = matmul(second_scaled, up_weight)
    gate_total, up_total, middle_square = (
        lax.psum(gate_part.astype(jnp.bfloat16), "kv").astype(jnp.float32),
        lax.psum(up_part.astype(jnp.bfloat16), "kv").astype(jnp.float32),
        lax.psum(sum_squares(middle_f).astype(jnp.bfloat16), "kv").astype(jnp.float32),
    )
    second_scale = lax.rsqrt(middle_square / model_width + epsilon)[:, None]
    hidden = (jax.nn.silu(second_scale * gate_total) * (second_scale * up_total)).astype(
        jnp.bfloat16
    )
    mixed = lax.psum_scatter(
        matmul(hidden, down_weight).astype(jnp.bfloat16), "tp", scatter_dimension=1, tiled=True
    ).astype(jnp.float32)
    share_width = mixed.shape[1]
    own_middle = lax.dynamic_slice_in_dim(
        middle_f, lax.axis_index("tp") * share_width, share_width, 1
    )
    return (own_middle + mixed).astype(jnp.bfloat16)


def solution(mesh):
    return jax.shard_map(
        local,
        mesh=mesh,
        in_specs=(
            P(None, ("kv", "tp")),
            P(("kv", "tp")),
            P(("kv", "tp"), None),
            P(("kv", "tp"), None),
            P(("kv", "tp"), None),
            P(),
            P(),
            P(None, "tp"),
            P(None, "tp"),
            P("tp", None, None),
            P("tp", None, None),
            P(None, "kv", None),
            P(None, "kv", None),
            P("tp"),
            P("tp", "kv"),
            P("kv"),
            P("kv", "tp"),
            P("kv", "tp"),
            P("tp", "kv"),
        ),
        out_specs=P(None, ("kv", "tp")),
        check_vma=False,
    )
```

profile of v0, /device:TPU:0, one launch (start us, length us, event | category | flops | bytes accessed | tf_op | source)
XLA Modules:
  0.0 365.7 jit_solution(8575871033755606622)
XLA Ops:
  6.5 2.0 fusion.32
  10.0 1.1 fusion.30
  11.1 0.9 fusion.28
  12.0 8.0 %all_gather.12 = bf16[24,512]{1,0:T(8,128)(2,1)} all-gather(bf16[24,128]{1,0:T(8,128)(2,1)} %param.19), channel_id=1, replica_groups=mesh['kv'=8,'tp'=4] {'tp'}, dimensions={1}, use_global_device_ids=true | all-gather | bytes 30720 | tf_op jit(solution)/shard_map/all_gather | solution.py:61
  20.0 40.5 %all-reduce = (f32[24]{0:T(128)S(1)}, f32[24,512]{1,0:T(8,128)S(1)}, f32[24,64]{1,0:T(8,128)S(1)}) all-reduce(f32[24]{0:T(128)S(1)} %fusion.26, f32[24,512]{1,0:T(8,128)S(1)} %fusion.30, f32[24,64]{1,0:T(8,128)S(1)} %fusion.28), channel_id=1, replica_groups=mesh['kv'=8,'tp'=4] {'kv','tp'}, use_global_device_ids=true, to_apply=%region_1.0 | all-reduce | flops 13848 | bytes 110784 | tf_op jit(solution)/shard_map/psum | solution.py:64
  63.0 75.0 %all-reduce.5.cloned.1.call-done = f32[24,1536]{1,0:T(8,128)} async-done(((f32[24,1536]{1,0:T(8,128)}), f32[24,1536]{1,0:T(8,128)}) %all-reduce.5.cloned.1.call-update) | async-done | bytes 147472 | tf_op jit(solution)/shard_map/psum | solution.py:64
  137.9 1.1 multiply_reduce_fusion.1
  139.1 1.5 fusion.38
  141.4 1.9 fusion.4
  143.6 4.6 %fusion.10 = f32[24,4,256]{2,1,0:T(4,128)S(1)} fusion(bf16[24,256,512]{2,1,0:T(8,128)(2,1)} %param.30, bf16[24,4,512]{2,0,1:T(8,128)(2,1)S(1)} %get-tuple-element.23), kind=kOutput, calls=%fused_computation.24 | convolution fusion | flops 25165824 | bytes 6488064 | tf_op jit(solution)/shard_map/bhc,bpc->bhp/dot_general | solution.py:92
  149.4 4.4 %convolution_convert_fusion.2 = bf16[24,4,512]{2,1,0:T(4,128)(2,1)} fusion(bf16[24,256,512]{2,1,0:T(8,128)(2,1)} %param.30, f32[24,4,256]{2,1,0:T(4,128)S(1)} %get-tuple-element.21, f32[24,4]{1,0:T(8,128)S(1)} %get-tuple-element.20), kind=kOutput, calls=%fused_computation.4 | convolution fusion | flops 25264128 | bytes 6488448 | tf_op jit(solution)/shard_map/bhp,bpc->bhc/dot_general | solution.py:98
  153.8 28.4 %all-gather.3 = f32[8,24,4]{1,2,0:T(4,128)S(1)} all-gather(f32[1,24,4]{1,2,0:T(4,128)S(1)} %bitcast.42), channel_id=2, replica_groups=mesh['kv'=8,'tp'=4] {'kv'}, dimensions={0}, use_global_device_ids=true | all-gather | bytes 3456 | tf_op jit(solution)/shard_map/all_gather | solution.py:102
  183.3 26.1 %all-gather.4 = f32[8,24,4]{1,2,0:T(4,128)S(1)} all-gather(f32[1,24,4]{1,2,0:T(4,128)S(1)} %bitcast.43), channel_id=4, replica_groups=mesh['kv'=8,'tp'=4] {'kv'}, dimensions={0}, use_global_device_ids=true | all-gather | bytes 3456 | tf_op jit(solution)/shard_map/all_gather | solution.py:103
  211.5 32.5 %all-gather.1 = bf16[192,4,512]{2,1,0:T(4,128)(2,1)S(1)} all-gather(bf16[24,4,512]{2,1,0:T(4,128)(2,1)} %convolution_convert_fusion.2), channel_id=3, replica_groups=mesh['kv'=8,'tp'=4] {'kv'}, dimensions={0}, use_global_device_ids=true | all-gather | bytes 884736 | tf_op jit(solution)/shard_map/all_gather | solution.py:119
  244.5 1.4 multiply_reduce_fusion.3
  246.1 10.3 %psum.68 = bf16[24,512]{1,0:T(8,128)(2,1)S(1)} all-reduce(bf16[24,512]{1,0:T(8,128)(2,1)S(1)} %convolution_convert_fusion.6), channel_id=1, replica_groups=mesh['kv'=8,'tp'=4] {'tp'}, use_global_device_ids=true, to_apply=%region_16.0 | all-reduce | flops 12288 | bytes 49152 | tf_op jit(solution)/shard_map/psum | solution.py:131
  256.4 6.3 %psum.67 = f32[24]{0:T(128)S(1)} all-reduce(f32[24]{0:T(128)S(1)} %get-tuple-element.24), channel_id=1, replica_groups=mesh['kv'=8,'tp'=4] {'tp'}, use_global_device_ids=true, to_apply=%region_15.0 | all-reduce | flops 24 | bytes 192 | tf_op jit(solution)/shard_map/psum | solution.py:128
  262.7 1.1 multiply_reduce_fusion.2
  263.8 1.8 convolution_convert_fusion
  265.6 1.1 convolution_convert_fusion.1
  266.8 18.2 %psum.69 = bf16[24]{0:T(256)(128)(2,1)S(1)} all-reduce(bf16[24]{0:T(256)(128)(2,1)S(1)} %get-tuple-element.10), channel_id=1, replica_groups=mesh['kv'=8,'tp'=4] {'kv'}, use_global_device_ids=true, to_apply=%region_18.0 | all-reduce | flops 24 | bytes 96 | tf_op jit(solution)/shard_map/psum | solution.py:142
  285.0 50.3 %all-reduce.7.cloned.1.call-done = (bf16[24,2816]{1,0:T(8,128)(2,1)}, bf16[24,2816]{1,0:T(8,128)(2,1)}) async-done(((bf16[24,2816]{1,0:T(8,128)(2,1)}, bf16[24,2816]{1,0:T(8,128)(2,1)}), (bf16[24,2816]{1,0:T(8,128)(2,1)}, bf16[24,2816]{1,0:T(8,128)(2,1)})) %all-reduce.7.cloned.1.call-update) | async-done | bytes 270352 | tf_op jit(solution)/shard_map/psum | solution.py:141
  335.3 2.5 convolution_convert_fusion.5
  338.6 19.1 %reduce-scatter.4.cloned.1.call-done = bf16[128,24]{1,0:T(8,128)(2,1)} async-done(((bf16[512,24]{1,0:T(8,128)(2,1)}), bf16[128,24]{1,0:T(8,128)(2,1)}) %reduce-scatter.4.cloned.1.call-update) | async-done | bytes 6160
  (57 shorter events, 12.4 us)
Async XLA Ops:
  6.5 257.2 %copy-start = (bf16[512,2816]{1,0:T(8,128)(2,1)S(1)}, bf16[512,2816]{1,0:T(8,128)(2,1)}, u32[]{:S(2)}) copy-start(bf16[512,2816]{1,0:T(8,128)(2,1)} %param.36) | copy-start | bytes 8650756
  6.5 136.8 %copy-start.4 = (bf16[4,128,512]{2,1,0:T(8,128)(2,1)S(1)}, bf16[4,128,512]{2,1,0:T(8,128)(2,1)}, u32[]{:S(2)}) copy-start(bf16[4,128,512]{2,1,0:T(8,128)(2,1)} %param.28) | copy-start | bytes 1572868
  6.5 131.4 %all-reduce.5.cloned.1.call-start = ((), (), s32[]{:S(2)}) async-start(), calls=%async_computation.1 | async-start | bytes 294912 | tf_op jit(solution)/shard_map/psum | solution.py:64
  8.6 326.8 %all-reduce.7.cloned.1.call-start = ((), (), s32[]{:S(2)}) async-start(), calls=%async_computation.3 | async-start | bytes 540672 | tf_op jit(solution)/shard_map/psum | solution.py:141
  60.5 80.1 %copy-start.6 = (f32[24]{0:T(128)}, f32[24]{0:T(128)S(1)}, u32[]{:S(2)}) copy-start(f32[24]{0:T(128)S(1)} %add_rsqrt_fusion.4) | copy-start | bytes 292
  139.1 1.5 copy-start.9
  143.6 4.6 %copy-start.2 = (bf16[24,256,64]{1,2,0:T(8,128)(2,1)S(1)}, bf16[24,256,64]{1,2,0:T(8,128)(2,1)}, u32[]{:S(2)}) copy-start(bf16[24,256,64]{1,2,0:T(8,128)(2,1)} %param.31) | copy-start | bytes 2359300
  149.4 32.8 %copy-start.5 = (f32[24,64]{1,0:T(8,128)S(1)}, f32[24,64]{1,0:T(8,128)}, u32[]{:S(2)}) copy-start(f32[24,64]{1,0:T(8,128)} %maximum_convert_fusion) | copy-start | bytes 18436
  153.8 92.1 %copy-start.3 = (bf16[512,512]{1,0:T(8,128)(2,1)S(1)}, bf16[512,512]{1,0:T(8,128)(2,1)}, u32[]{:S(2)}) copy-start(bf16[512,512]{1,0:T(8,128)(2,1)} %param.33) | copy-start | bytes 1572868
  211.5 34.5 %copy-start.8 = (f32[512]{0:T(512)S(1)}, f32[512]{0:T(512)}, u32[]{:S(2)}) copy-start(f32[512]{0:T(512)} %param.32) | copy-start | bytes 6148
  244.5 21.1 %copy-start.7 = (f32[512]{0:T(512)S(1)}, f32[512]{0:T(512)}, u32[]{:S(2)}) copy-start(f32[512]{0:T(512)} %param.34) | copy-start | bytes 6148
  262.7 2.9 copy-start.1
  266.8 90.9 %reduce-scatter.4.cloned.1.call-start = ((), (), s32[]{:S(2)}) async-start(), calls=%async_computation.2 | async-start | bytes 163840
Sparse Core Ops, SparseCore 0:
  12.9 125.0 all-reduce.4
  266.9 68.3 all-reduce.6
  338.8 18.9 reduce-scatter.3
where the time goes:
time: 367 us; the launch traced here: 366 us
  blocking collectives  170 us (46%)
  waiting for transfers between devices  144 us (39%)
  matrix products  24.1 us (7%)
  between operations  13.2 us (4%)
  other arithmetic  10.1 us (3%)
    psum x1, waiting for transfers between devices, local(): lax.psum((matmul(first_scaled, query_down), matmul(first_scaled, latent_d...  75 us
    psum x1, waiting for transfers between devices, local(): lax.psum(up_part.astype(jnp.bfloat16), 'kv').astype(jnp.float32)  50.3 us
    psum x1, blocking collectives, local(): lax.psum((matmul(first_scaled, query_down), matmul(first_scaled, latent_d...  40.5 us
    all_gather x1, blocking collectives, local(): lax.all_gather(weighted[None], 'kv', axis=0, tiled=True).astype(jnp.float32)  32.5 us
    all_gather x1, blocking collectives, local(): lax.all_gather(maxima[None], 'kv', axis=0, tiled=True)  28.4 us
    all_gather x1, blocking collectives, local(): lax.all_gather(totals[None], 'kv', axis=0, tiled=True)  26.1 us
    unnamed x4, waiting for transfers between devices  19.1 us
    psum x1, blocking collectives, local(): lax.psum(sum_squares(middle_f).astype(jnp.bfloat16), 'kv')  18.2 us
  transfers between devices with their start and end apart: 3, of which 3 were waited for; matrix products, arithmetic and copies ran while one was open for 2% of the time, Pallas kernels for 0%

commit v1 on v0

--- a/solution.py
+++ b/solution.py
@@ -138,7 +138,7 @@
     up_part = matmul(second_scaled, up_weight)
     gate_total, up_total, middle_square = (
         lax.psum(gate_part.astype(jnp.bfloat16), "kv").astype(jnp.float32),
-        lax.psum(up_part.astype(jnp.bfloat16), "kv").astype(jnp.float32),
+        jnp.sum(lax.all_gather(up_part.astype(jnp.bfloat16), "kv"), axis=0).astype(jnp.float32),
         lax.psum(sum_squares(middle_f).astype(jnp.bfloat16), "kv").astype(jnp.float32),
     )
     second_scale = lax.rsqrt(middle_square / model_width + epsilon)[:, None]

time: 367 us -> 407 us (1.11)
  waiting for transfers between devices: 144 us -> 182 us
    psum x1, waiting for transfers between devices: 50.3 us -> 71.1 us  [local(): lax.psum(gate_part.astype(jnp.bfloat16), 'kv').astype(jnp.float32)]
    all_gather x0 -> x1, waiting for transfers between devices: none -> 16.5 us  [local(): lax.all_gather(up_part.astype(jnp.bfloat16), 'kv')]
    unnamed x4 -> x5, waiting for transfers between devices: 19.1 us -> 18.9 us
  transfers between devices with their start and end apart: 3 -> 4, of which waited for: 3 -> 4; matrix products, arithmetic and copies ran while one was open for 2% -> 3% of each run, Pallas kernels for 0% -> 0%
where the time goes in v1:
time: 407 us; the launch traced here: 406 us
  waiting for transfers between devices  182 us (45%)
  blocking collectives  170 us (42%)
  matrix products  25.8 us (6%)
  between operations  13.3 us (3%)
  other arithmetic  11.4 us (3%)
    psum x1, waiting for transfers between devices, local(): lax.psum((matmul(first_scaled, query_down), matmul(first_scaled, latent_d...  75 us
    psum x1, waiting for transfers between devices, local(): lax.psum(gate_part.astype(jnp.bfloat16), 'kv').astype(jnp.float32)  71.1 us
    psum x1, blocking collectives, local(): lax.psum((matmul(first_scaled, query_down), matmul(first_scaled, latent_d...  40.4 us
    all_gather x1, blocking collectives, local(): lax.all_gather(weighted[None], 'kv', axis=0, tiled=True).astype(jnp.float32)  32.5 us
    all_gather x1, blocking collectives, local(): lax.all_gather(maxima[None], 'kv', axis=0, tiled=True)  28.4 us
    all_gather x1, blocking collectives, local(): lax.all_gather(totals[None], 'kv', axis=0, tiled=True)  26.1 us
    unnamed x5, waiting for transfers between devices  18.9 us
    psum x1, blocking collectives, local(): lax.psum(sum_squares(middle_f).astype(jnp.bfloat16), 'kv')  18.1 us
  transfers between devices with their start and end apart: 4, of which 4 were waited for; matrix products, arithmetic and copies ran while one was open for 3% of the time, Pallas kernels for 0%

profile of v1, /device:TPU:0, one launch (start us, length us, event | category | flops | bytes accessed | tf_op | source)
XLA Modules:
  0.0 405.7 jit_solution(13791331316202314132)
XLA Ops:
  6.5 2.0 fusion.32
  10.0 1.1 fusion.30
  12.0 8.0 %all_gather.18 = bf16[24,512]{1,0:T(8,128)(2,1)} all-gather(bf16[24,128]{1,0:T(8,128)(2,1)} %param.19), channel_id=1, replica_groups=mesh['kv'=8,'tp'=4] {'tp'}, dimensions={1}, use_global_device_ids=true | all-gather | bytes 30720 | tf_op jit(solution)/shard_map/all_gather | solution.py:61
  20.0 40.4 %all-reduce = (f32[24]{0:T(128)S(1)}, f32[24,512]{1,0:T(8,128)S(1)}, f32[24,64]{1,0:T(8,128)S(1)}) all-reduce(f32[24]{0:T(128)S(1)} %fusion.26, f32[24,512]{1,0:T(8,128)S(1)} %fusion.30, f32[24,64]{1,0:T(8,128)S(1)} %fusion.28), channel_id=1, replica_groups=mesh['kv'=8,'tp'=4] {'kv','tp'}, use_global_device_ids=true, to_apply=%region_1.0 | all-reduce | flops 13848 | bytes 110784 | tf_op jit(solution)/shard_map/psum | solution.py:64
  62.9 75.0 %all-reduce.4.cloned.1.call-done = f32[24,1536]{1,0:T(8,128)} async-done(((f32[24,1536]{1,0:T(8,128)}), f32[24,1536]{1,0:T(8,128)}) %all-reduce.4.cloned.1.call-update) | async-done | bytes 147472 | tf_op jit(solution)/shard_map/psum | solution.py:64
  137.9 1.1 multiply_reduce_fusion.1
  139.1 1.5 fusion.38
  141.4 1.9 fusion.4
  143.6 4.6 %fusion.10 = f32[24,4,256]{2,1,0:T(4,128)S(1)} fusion(bf16[24,256,512]{2,1,0:T(8,128)(2,1)} %param.30, bf16[24,4,512]{2,0,1:T(8,128)(2,1)S(1)} %get-tuple-element.21), kind=kOutput, calls=%fused_computation.24 | convolution fusion | flops 25165824 | bytes 6488064 | tf_op jit(solution)/shard_map/bhc,bpc->bhp/dot_general | solution.py:92
  149.4 4.4 %convolution_convert_fusion.2 = bf16[24,4,512]{2,1,0:T(4,128)(2,1)} fusion(bf16[24,256,512]{2,1,0:T(8,128)(2,1)} %param.30, f32[24,4,256]{2,1,0:T(4,128)S(1)} %get-tuple-element.19, f32[24,4]{1,0:T(8,128)S(1)} %get-tuple-element.18), kind=kOutput, calls=%fused_computation.4 | convolution fusion | flops 25264128 | bytes 6488448 | tf_op jit(solution)/shard_map/bhp,bpc->bhc/dot_general | solution.py:98
  153.8 28.4 %all-gather.4 = f32[8,24,4]{1,2,0:T(4,128)S(1)} all-gather(f32[1,24,4]{1,2,0:T(4,128)S(1)} %bitcast.44), channel_id=2, replica_groups=mesh['kv'=8,'tp'=4] {'kv'}, dimensions={0}, use_global_device_ids=true | all-gather | bytes 3456 | tf_op jit(solution)/shard_map/all_gather | solution.py:102
  183.3 26.1 %all-gather.5 = f32[8,24,4]{1,2,0:T(4,128)S(1)} all-gather(f32[1,24,4]{1,2,0:T(4,128)S(1)} %bitcast.45), channel_id=4, replica_groups=mesh['kv'=8,'tp'=4] {'kv'}, dimensions={0}, use_global_device_ids=true | all-gather | bytes 3456 | tf_op jit(solution)/shard_map/all_gather | solution.py:103
  211.5 32.5 %all-gather.1 = bf16[192,4,512]{2,1,0:T(4,128)(2,1)S(1)} all-gather(bf16[24,4,512]{2,1,0:T(4,128)(2,1)} %convolution_convert_fusion.2), channel_id=3, replica_groups=mesh['kv'=8,'tp'=4] {'kv'}, dimensions={0}, use_global_device_ids=true | all-gather | bytes 884736 | tf_op jit(solution)/shard_map/all_gather | solution.py:119
  244.5 1.4 multiply_reduce_fusion.3
  246.1 10.3 %psum.61 = bf16[24,512]{1,0:T(8,128)(2,1)S(1)} all-reduce(bf16[24,512]{1,0:T(8,128)(2,1)S(1)} %convolution_convert_fusion.6), channel_id=1, replica_groups=mesh['kv'=8,'tp'=4] {'tp'}, use_global_device_ids=true, to_apply=%region_16.0 | all-reduce | flops 12288 | bytes 49152 | tf_op jit(solution)/shard_map/psum | solution.py:131
  256.4 6.3 %psum.60 = f32[24]{0:T(128)S(1)} all-reduce(f32[24]{0:T(128)S(1)} %get-tuple-element.22), channel_id=1, replica_groups=mesh['kv'=8,'tp'=4] {'tp'}, use_global_device_ids=true, to_apply=%region_15.0 | all-reduce | flops 24 | bytes 192 | tf_op jit(solution)/shard_map/psum | solution.py:128
  263.6 1.8 convolution_convert_fusion
  265.5 18.1 %psum.62 = bf16[24]{0:T(256)(128)(2,1)S(1)} all-reduce(bf16[24]{0:T(256)(128)(2,1)S(1)} %get-tuple-element.8), channel_id=1, replica_groups=mesh['kv'=8,'tp'=4] {'kv'}, use_global_device_ids=true, to_apply=%region_18.0 | all-reduce | flops 24 | bytes 96 | tf_op jit(solution)/shard_map/psum | solution.py:142
  283.6 3.0 convolution_convert_fusion.1
  286.7 16.5 %all-gather.8.cloned.1.call-done = bf16[192,2816]{1,0:T(8,128)(2,1)} async-done(((bf16[24,2816]{1,0:T(8,128)(2,1)}), bf16[192,2816]{1,0:T(8,128)(2,1)}) %all-gather.8.cloned.1.call-update) | async-done | bytes 1081360 | tf_op jit(solution)/shard_map/all_gather | solution.py:141
  303.2 1.4 reduce_sum.112
  304.6 71.1 %all-reduce.6.cloned.1.call-done = bf16[24,2816]{1,0:T(8,128)(2,1)} async-done(((bf16[24,2816]{1,0:T(8,128)(2,1)}), bf16[24,2816]{1,0:T(8,128)(2,1)}) %all-reduce.6.cloned.1.call-update) | async-done | bytes 135184 | tf_op jit(solution)/shard_map/psum | solution.py:140
  375.7 2.5 convolution_convert_fusion.5
  378.9 18.9 %reduce-scatter.4.cloned.1.call-done = bf16[128,24]{1,0:T(8,128)(2,1)} async-done(((bf16[512,24]{1,0:T(8,128)(2,1)}), bf16[128,24]{1,0:T(8,128)(2,1)}) %reduce-scatter.4.cloned.1.call-update) | async-done | bytes 6160
  (59 shorter events, 14.2 us)
Async XLA Ops:
  6.5 257.1 %copy-start = (bf16[512,2816]{1,0:T(8,128)(2,1)S(1)}, bf16[512,2816]{1,0:T(8,128)(2,1)}, u32[]{:S(2)}) copy-start(bf16[512,2816]{1,0:T(8,128)(2,1)} %param.36) | copy-start | bytes 8650756
  6.5 136.8 %copy-start.3 = (bf16[4,128,512]{2,1,0:T(8,128)(2,1)S(1)}, bf16[4,128,512]{2,1,0:T(8,128)(2,1)}, u32[]{:S(2)}) copy-start(bf16[4,128,512]{2,1,0:T(8,128)(2,1)} %param.28) | copy-start | bytes 1572868
  6.5 131.4 %all-reduce.4.cloned.1.call-start = ((), (), s32[]{:S(2)}) async-start(), calls=%async_computation.1 | async-start | bytes 294912 | tf_op jit(solution)/shard_map/psum | solution.py:64
  8.6 294.6 %all-gather.8.cloned.1.call-start = ((), (), s32[]{:S(2)}) async-start(), calls=%async_computation.3 | async-start | bytes 1216512 | tf_op jit(solution)/shard_map/all_gather | solution.py:141
  60.5 80.1 %copy-start.5 = (f32[24]{0:T(128)}, f32[24]{0:T(128)S(1)}, u32[]{:S(2)}) copy-start(f32[24]{0:T(128)S(1)} %add_rsqrt_fusion.4) | copy-start | bytes 292
  139.1 1.5 copy-start.8
  143.6 4.6 %copy-start.1 = (bf16[24,256,64]{1,2,0:T(8,128)(2,1)S(1)}, bf16[24,256,64]{1,2,0:T(8,128)(2,1)}, u32[]{:S(2)}) copy-start(bf16[24,256,64]{1,2,0:T(8,128)(2,1)} %param.31) | copy-start | bytes 2359300
  149.4 32.8 %copy-start.4 = (f32[24,64]{1,0:T(8,128)S(1)}, f32[24,64]{1,0:T(8,128)}, u32[]{:S(2)}) copy-start(f32[24,64]{1,0:T(8,128)} %maximum_convert_fusion) | copy-start | bytes 18436
  153.8 92.1 %copy-start.2 = (bf16[512,512]{1,0:T(8,128)(2,1)S(1)}, bf16[512,512]{1,0:T(8,128)(2,1)}, u32[]{:S(2)}) copy-start(bf16[512,512]{1,0:T(8,128)(2,1)} %param.33) | copy-start | bytes 1572868
  211.5 34.5 %copy-start.7 = (f32[512]{0:T(512)S(1)}, f32[512]{0:T(512)}, u32[]{:S(2)}) copy-start(f32[512]{0:T(512)} %param.32) | copy-start | bytes 6148
  244.5 39.1 %copy-start.6 = (f32[512]{0:T(512)S(1)}, f32[512]{0:T(512)}, u32[]{:S(2)}) copy-start(f32[512]{0:T(512)} %param.34) | copy-start | bytes 6148
  265.5 110.2 %all-reduce.6.cloned.1.call-start = ((), (), s32[]{:S(2)}) async-start(), calls=%async_computation.2 | async-start | bytes 270336 | tf_op jit(solution)/shard_map/psum | solution.py:140
  286.6 111.2 %reduce-scatter.4.cloned.1.call-start = ((), (), s32[]{:S(2)}) async-start(), calls=%async_computation.4 | async-start | bytes 163840
Sparse Core Ops, SparseCore 0:
  12.9 125.0 all-reduce.3
  265.6 37.5 all-gather.7
  306.5 69.0 all-reduce.5
  379.0 18.7 reduce-scatter.3
